TPU v7x, 256 devices: a whole 4x4x8 slice. The times are simulated.
256 devices in a mesh: gr: 2 (over z_hi), sp: 16 (over z_lo, y), tp: 8 (over x, core).
Axes of the slice: x: 4, y: 4, z: 8 (z_hi: 2, z_lo: 4; z = z_hi * 4 + z_lo), core: 2. Of those that a mesh axis runs over, the one named last changes fastest.
Arguments:
- tokens: bfloat16 [8, 3072, 4096], P('gr', 'sp', 'tp'), may hold values from -6.5 to 6.5
- first_token_input: bfloat16 [8, 4096], P('gr', 'sp'), may hold values from -6 to 6
- forget_weight: bfloat16 [4096, 4096], P(None, 'tp'), may hold values from -0.1171875 to 0.1171875
- value_weight: bfloat16 [4096, 4096], P(None, 'tp'), may hold values from -0.375 to 0.375
- query_weight: bfloat16 [4096, 4096], P('sp', 'tp'), may hold values from -0.09375 to 0.09375
- output_gate_weight: bfloat16 [4096, 4096], P('sp', 'tp'), may hold values from -0.09375 to 0.09375
- forget_bound_slack: float32 [4096], P('tp'), may hold values from 0.00016276042 to 0.8, as said below
- additional_damping_exponent: float32 [8, 3072, 32], P('gr', 'sp', 'tp'), may hold values from -2.2 to 0, as said below
- read_norm_scale: float32 [128], replicated, may hold values from 0.1 to 1.9
Outputs:
- cache: bfloat16 [8, 32, 128, 128], P('gr', 'tp', 'sp')
- first_read: bfloat16 [8, 4096], P('gr', 'tp')
Inputs may be any that keep to these rules, and one draw needn't show every extreme that they name: `forget_bound_slack`: positive gaps, one per channel. `additional_damping_exponent`: non-positive log-decays.
All inputs are finite; a program needn't handle non-finite values.
Results may differ from a plain program's by a relative error of at most 0.018.
Values may be sent and summed in bfloat16 or wider, within the bound.
A program may use at most 64 MiB of HBM per device.

v0:
```python
import jax
import jax.numpy as jnp
from jax import lax
from jax.sharding import PartitionSpec as P


def from_everyone(shard, axis):
    count = lax.axis_size(axis)
    return lax.all_to_all(
        jnp.broadcast_to(shard[None], (count, *shard.shape)), axis, 0, 0, tiled=True
    )


def folded_in_pairs(pieces, combine):
    while len(jax.tree.leaves(pieces)[0]) > 1:
        pieces = jax.vmap(combine)(*(pieces[side::2] for side in (0, 1)))
    return pieces[0]


def prefix(shard, axis, combine, identity):
    count, position = (lax.axis_size(axis), lax.axis_index(axis))
    passed = jnp.arange(count) > position

    def kept(part, zero, own):
        part = jnp.where(
            passed.reshape(-1, *(1 for _ in own.shape)), part, jnp.asarray(zero, own.dtype)
        )
        return part[::-1]

    pieces = from_everyone(shard, axis)
    return folded_in_pairs(kept(pieces, identity, shard), combine)


def cut_along(shard, dim, count):
    shape = shard.shape
    blocks = shard.reshape(*shape[:dim], count, shape[dim] // count, *shape[dim + 1 :])
    return jnp.moveaxis(blocks, dim, 0)


def sent_and_summed(shard, axis, dim):
    count = lax.axis_size(axis)
    blocks = lax.all_to_all(cut_along(shard, dim, count), axis, 0, 0, tiled=True)
    return jnp.sum(blocks.astype(jnp.float32), axis=0)


def of_everyone(shard, axis):
    everything = from_everyone(shard, axis)
    return jnp.sum(everything, axis=0)


def packed_total(arrays, axis):
    ends = [0]
    for a in arrays:
        ends.append(ends[-1] + a.size)
    total = of_everyone(jnp.concatenate([a.ravel() for a in arrays]), axis)
    return tuple((total[b:e].reshape(a.shape) for a, b, e in zip(arrays, ends, ends[1:])))


def add_sums(earlier, later_part):
    return earlier + later_part


def per_device(
    tokens,
    first_token_input,
    forget_weight,
    value_weight,
    query_weight,
    output_gate_weight,
    forget_bound_slack,
    additional_damping_exponent,
    read_norm_scale,
):
    seq_count, block_len, width_part = tokens.shape
    head_dim = read_norm_scale.shape[0]
    local_heads = additional_damping_exponent.shape[2]
    channels = local_heads * head_dim
    flat_rows = tokens.reshape(seq_count * block_len, width_part)
    segment = lax.all_gather(flat_rows, "tp", axis=1, tiled=True)
    forget_acc = jnp.dot(segment, forget_weight, preferred_element_type=jnp.float32)
    value_acc = jnp.dot(segment, value_weight, preferred_element_type=jnp.float32)
    forget = forget_acc.astype(jnp.bfloat16).reshape(seq_count, block_len, channels)
    values = value_acc.astype(jnp.bfloat16).reshape(seq_count, block_len, local_heads, head_dim)
    sp_count = lax.axis_size("sp")
    rows_here = head_dim // sp_count
    row_start = lax.axis_index("sp") * rows_here
    valve_sampler_seeds = forget_bound_slack * jax.nn.sigmoid(-forget.astype(jnp.float32))
    damping_exponent = jnp.log1p(-valve_sampler_seeds) + jnp.repeat(
        additional_damping_exponent, head_dim, axis=2
    )
    totals = jnp.sum(damping_exponent, axis=1)
    later_sum = prefix(totals, "sp", add_sums, jnp.zeros_like(totals))
    within = totals[:, None, :] - jnp.cumsum(damping_exponent, axis=1)
    weighted = (valve_sampler_seeds * jnp.exp(within + later_sum[:, None, :])).astype(jnp.bfloat16)
    weighted = weighted.reshape(seq_count, block_len, local_heads, head_dim)
    state_terms = jnp.einsum(
        "slha,slhb->shab", weighted, values, preferred_element_type=jnp.float32
    )
    state_sum = sent_and_summed(state_terms.astype(jnp.bfloat16), "sp", 2)
    cache_rows = state_sum.astype(jnp.bfloat16)
    slab_rows = first_token_input.shape[1]
    row_first = lax.axis_index("sp") * slab_rows
    forget_rows = lax.dynamic_slice_in_dim(forget_weight, row_first, slab_rows, 0)
    value_rows = lax.dynamic_slice_in_dim(value_weight, row_first, slab_rows, 0)
    new_sums = packed_total(
        (
            jnp.dot(first_token_input, query_weight, preferred_element_type=jnp.float32),
            jnp.dot(first_token_input, output_gate_weight, preferred_element_type=jnp.float32),
            jnp.dot(first_token_input, forget_rows, preferred_element_type=jnp.float32),
            jnp.dot(first_token_input, value_rows, preferred_element_type=jnp.float32),
        ),
        "sp",
    )
    new_query, new_gate, new_forget, new_value = [
        summed.astype(jnp.bfloat16) for summed in new_sums
    ]
    new_keys = (forget_bound_slack * jax.nn.sigmoid(-new_forget.astype(jnp.float32))).reshape(
        seq_count, local_heads, head_dim
    )
    own_keys = lax.dynamic_slice_in_dim(new_keys, row_start, rows_here, 2)
    own_query = lax.dynamic_slice_in_dim(
        new_query.astype(jnp.float32).reshape(seq_count, local_heads, head_dim),
        row_start,
        rows_here,
        2,
    )
    value_new = new_value.astype(jnp.float32).reshape(seq_count, local_heads, head_dim)
    updated = (1.0 - own_keys)[..., None] * cache_rows.astype(jnp.float32) + own_keys[
        ..., None
    ] * value_new[:, :, None, :]
    read_part = jnp.einsum("sha,shab->shb", own_query, updated, precision=lax.Precision.HIGHEST)
    read_sum = of_everyone(read_part, "sp")
    scaled = (
        read_sum
        * lax.rsqrt(jnp.mean(read_sum * read_sum, axis=-1, keepdims=True) + 1e-06)
        * read_norm_scale
    )
    first_read = (
        scaled.reshape(seq_count, channels) * jax.nn.silu(new_gate.astype(jnp.float32))
    ).astype(jnp.bfloat16)
    return (cache_rows, first_read)


def solution(mesh):
    placed = (
        P("gr", "sp", "tp"),
        P("gr", "sp"),
        P(None, "tp"),
        P(None, "tp"),
        P("sp", "tp"),
        P("sp", "tp"),
        P("tp"),
        P("gr", "sp", "tp"),
        P(),
    )
    return jax.shard_map(
        per_device,
        mesh=mesh,
        in_specs=placed,
        out_specs=(P("gr", "tp", "sp", None), P("gr", "tp")),
        check_vma=False,
    )
```

profile of v0, /device:TPU:1, one launch (start us, length us, event | category | flops | bytes accessed | tf_op | source)
XLA Modules:
  0.0 156.0 jit_solution(15677566617659732985)
XLA Ops:
  8.9 1.1 convolution_bitcast_fusion.2
  10.1 1.1 convolution_bitcast_fusion.1
  11.2 1.1 convolution_bitcast_fusion
  12.5 1.0 broadcast_in_dim.20
  13.5 1.8 %reshape.149 = f32[4,192,512]{2,1,0:T(8,128)} reshape(f32[4,192,4,128]{3,2,1,0:T(4,128)S(1)} %broadcast_in_dim.20) | data formatting | bytes 3145728 | tf_op jit(solution)/shard_map/reshape | solution.py:88
  15.3 42.2 %all-gather.2.cloned.1.call-done = bf16[768,4096]{1,0:T(8,128)(2,1)} async-done(((bf16[768,512]{1,0:T(8,128)(2,1)}), bf16[768,4096]{1,0:T(8,128)(2,1)}) %all-gather.2.cloned.1.call-update) | async-done | bytes 6291472 | tf_op jit(solution)/shard_map/all_gather | solution.py:79
  57.4 7.4 %convolution_convert_fusion = bf16[768,512]{1,0:T(8,128)(2,1)S(1)} fusion(bf16[768,4096]{1,0:T(8,128)(2,1)} %all-gather.2.cloned.1.call-done, bf16[4096,512]{1,0:T(8,128)(2,1)} %param.12), kind=kOutput, calls=%fused_computation.10 | convolution fusion | flops 3221618688 | bytes 11272192 | tf_op jit(solution)/shard_map/dot_general | solution.py:81
  64.9 1.1 reshape.153
  66.0 7.0 %add_divide_fusion = f32[768,512]{1,0:T(8,128)S(1)} fusion(bf16[768,4096]{1,0:T(8,128)(2,1)} %all-gather.2.cloned.1.call-done, bf16[4096,512]{1,0:T(8,128)(2,1)} %param.11), kind=kOutput, calls=%fused_computation.9 | convolution fusion | flops 3222798336 | bytes 12058624 | tf_op jit(solution)/shard_map/dot_general | solution.py:80
  73.7 2.4 %add_reduce_fusion = f32[4,4,128]{2,1,0:T(4,128)S(1)} fusion(f32[4,192,4,128]{3,2,1,0:T(4,128)S(1)} %div.22, f32[4,192,4]{2,1,0:T(8,128)} %copy-done.2, f32[4,128]{1,0:T(4,128)S(1)} %bitcast.77), kind=kLoop, calls=%fused_computation.8 | loop fusion | flops 1570816 | bytes 1595392 | tf_op jit(solution)/shard_map/reduce_sum | solution.py:91
  76.8 7.1 %all-to-all-start = ((f32[16,4,512]{2,1,0:T(4,128)}), f32[16,4,512]{2,1,0:T(4,128)S(1)}, u32[]{:S(2)}, u32[]{:S(2)}) async-start(f32[16,4,512]{2,1,0:T(4,128)} %broadcast_in_dim.22), calls=%async_computation | async-start | bytes 262144 | tf_op jit(solution)/shard_map/all_to_all | solution.py:9
  83.9 2.0 %add_bitcast_fusion = f32[4,512,192]{1,2,0:T(8,128)S(1)} fusion(f32[4,192,512]{2,1,0:T(8,128)} %reshape.149, f32[4,192,512]{2,1,0:T(8,128)S(1)} %bitcast.70, f32[512]{0:T(512)S(1)} %copy-done.5), kind=kLoop, calls=%fused_computation.7 | loop fusion | flops 1179648 | bytes 4720640 | tf_op jit(solution)/shard_map/transpose
  86.1 1.6 %fusion = f32[4,512,2,128]{1,2,3,0:T(2,128)S(1)} fusion(f32[4,512,2,128]{1,3,2,0:T(8,128)S(1)} %bitcast.72), kind=kOutput, calls=%fused_computation | output fusion | flops 66584576 | bytes 4194304 | tf_op jit(solution)/shard_map/reduce-window
  87.8 1.3 copy-done.1
  89.2 2.3 %broadcast_add_fusion = f32[4,512,2,128]{1,2,3,0:T(2,128)S(1)} fusion(f32[4,512,2,128]{1,2,3,0:T(2,128)} %copy-done.1, f32[4,512,2]{1,2,0:T(2,128)S(1)} %slice.107), kind=kLoop, calls=%fused_computation.18 | loop fusion | flops 524288 | bytes 4210688 | tf_op jit(solution)/shard_map/reduce_window_sum
  91.5 1.7 %copy.32 = f32[4,512,2,128]{1,3,2,0:T(8,128)} copy(f32[4,512,2,128]{1,2,3,0:T(2,128)S(1)} %broadcast_add_fusion) | data formatting | bytes 4194304 | tf_op jit(solution)/shard_map/reduce_window_sum
  93.2 1.2 broadcast_in_dim.24
  94.4 7.0 %all-to-all-start.2 = ((f32[16,1,8192]{2,1,0:T(1,128)}), f32[16,1,8192]{2,1,0:T(1,128)S(1)}, u32[]{:S(2)}, u32[]{:S(2)}) async-start(f32[16,1,8192]{2,1,0:T(1,128)} %broadcast_in_dim.24), calls=%async_computation.2 | async-start | bytes 1048576 | tf_op jit(solution)/shard_map/all_to_all | solution.py:9
  101.6 2.1 %fusion.6 = bf16[4,4,16,8,128]{4,3,2,1,0:T(8,128)(2,1)S(1)} fusion(bf16[4,192,4,128]{3,2,1,0:T(4,128)(2,1)S(1)} %copy-done.3, f32[4,256,512]{2,1,0:T(8,128)} %bitcast.73, f32[4,192,512]{2,1,0:T(8,128)S(1)} %bitcast.71, f32[4,512]{1,0:T(4,128)S(1)} %fusion.22, f32[4,512]{1,0:T(4,128)S(1)} %bitcast.76, f32[512]{0:T(512)S(1)} %copy-done.5), kind=kOutput, calls=%fused_computation.13 | convolution fusion | flops 102891520 | bytes 4474880 | tf_op jit(solution)/shard_map/slha,slhb->shab/dot_general | solution.py:96
  104.6 10.5 %all-to-all-done.2 = f32[16,1,8192]{2,1,0:T(1,128)S(1)} async-done(((f32[16,1,8192]{2,1,0:T(1,128)}), f32[16,1,8192]{2,1,0:T(1,128)S(1)}, u32[]{:S(2)}, u32[]{:S(2)}) %all-to-all-start.2) | async-done | bytes 524320 | tf_op jit(solution)/shard_map/all_to_all | solution.py:9
  115.1 5.5 %all-to-all-start.1 = ((bf16[16,4,4,8,128]{4,3,2,1,0:T(8,128)(2,1)}), bf16[16,4,4,8,128]{4,3,2,1,0:T(8,128)(2,1)S(1)}, u32[]{:S(2)}, u32[]{:S(2)}) async-start(bf16[16,4,4,8,128]{4,3,2,1,0:T(8,128)(2,1)} %bitcast.68), calls=%async_computation.1 | async-start | bytes 1048576 | tf_op jit(solution)/shard_map/all_to_all | solution.py:42
  121.3 12.6 %all-to-all-done.1 = bf16[16,4,4,8,128]{4,3,2,1,0:T(8,128)(2,1)S(1)} async-done(((bf16[16,4,4,8,128]{4,3,2,1,0:T(8,128)(2,1)}), bf16[16,4,4,8,128]{4,3,2,1,0:T(8,128)(2,1)S(1)}, u32[]{:S(2)}, u32[]{:S(2)}) %all-to-all-start.1) | async-done | bytes 524320 | tf_op jit(solution)/shard_map/all_to_all | solution.py:42
  134.9 5.6 %all-to-all-start.3 = ((f32[16,4,4,128]{3,2,1,0:T(4,128)}), f32[16,4,4,128]{3,2,1,0:T(4,128)S(1)}, u32[]{:S(2)}, u32[]{:S(2)}) async-start(f32[16,4,4,128]{3,2,1,0:T(4,128)} %broadcast_in_dim.25), calls=%async_computation.3 | async-start | bytes 262144 | tf_op jit(solution)/shard_map/all_to_all | solution.py:9
  140.5 7.8 %all-to-all-done.3 = f32[16,4,4,128]{3,2,1,0:T(4,128)S(1)} async-done(((f32[16,4,4,128]{3,2,1,0:T(4,128)}), f32[16,4,4,128]{3,2,1,0:T(4,128)S(1)}, u32[]{:S(2)}, u32[]{:S(2)}) %all-to-all-start.3) | async-done | bytes 131104 | tf_op jit(solution)/shard_map/all_to_all | solution.py:9
  (61 shorter events, 7.2 us)
Async XLA Ops:
  7.2 1.0 copy-start
  7.2 4.0 %copy-start.4 = (bf16[4,256]{1,0:T(4,128)(2,1)S(1)}, bf16[4,256]{1,0:T(4,128)(2,1)}, u32[]{:S(2)}) copy-start(bf16[4,256]{1,0:T(4,128)(2,1)} %param.10) | copy-start | bytes 6148
  7.2 5.1 %copy-start.7 = (f32[4,192,4]{1,2,0:T(4,128)S(1)}, f32[4,192,4]{1,2,0:T(4,128)}, u32[]{:S(2)}) copy-start(f32[4,192,4]{1,2,0:T(4,128)} %param.16) | copy-start | bytes 36868
  7.2 50.2 %all-gather.2.cloned.1.call-start = ((), (), s32[]{:S(2)}) async-start(), calls=%async_computation.4 | async-start | bytes 7077888 | tf_op jit(solution)/shard_map/all_gather | solution.py:79
  12.5 2.8 %copy-start.2 = (f32[4,192,4]{2,1,0:T(8,128)}, f32[4,192,4]{2,1,0:T(8,128)S(1)}, u32[]{:S(2)}) copy-start(f32[4,192,4]{2,1,0:T(8,128)S(1)} %copy.30) | copy-start | bytes 36868
  73.0 0.7 copy-start.5
  76.8 16.5 %all-to-all-start = ((f32[16,4,512]{2,1,0:T(4,128)}), f32[16,4,512]{2,1,0:T(4,128)S(1)}, u32[]{:S(2)}, u32[]{:S(2)}) async-start(f32[16,4,512]{2,1,0:T(4,128)} %broadcast_in_dim.22), calls=%async_computation | async-start | bytes 262144 | tf_op jit(solution)/shard_map/all_to_all | solution.py:9
  87.8 1.3 copy-start.1
  93.2 8.4 %copy-start.3 = (bf16[4,192,4,128]{3,2,1,0:T(4,128)(2,1)S(1)}, bf16[4,192,4,128]{3,2,1,0:T(4,128)(2,1)}, u32[]{:S(2)}) copy-start(bf16[4,192,4,128]{3,2,1,0:T(4,128)(2,1)} %reshape.153) | copy-start | bytes 2359300
  94.4 20.6 %all-to-all-start.2 = ((f32[16,1,8192]{2,1,0:T(1,128)}), f32[16,1,8192]{2,1,0:T(1,128)S(1)}, u32[]{:S(2)}, u32[]{:S(2)}) async-start(f32[16,1,8192]{2,1,0:T(1,128)} %broadcast_in_dim.24), calls=%async_computation.2 | async-start | bytes 1048576 | tf_op jit(solution)/shard_map/all_to_all | solution.py:9
  115.1 25.4 %copy-start.8 = (f32[128]{0:T(128)S(1)}, f32[128]{0:T(128)}, u32[]{:S(2)}) copy-start(f32[128]{0:T(128)} %param.17) | copy-start | bytes 1540
  115.1 18.7 %all-to-all-start.1 = ((bf16[16,4,4,8,128]{4,3,2,1,0:T(8,128)(2,1)}), bf16[16,4,4,8,128]{4,3,2,1,0:T(8,128)(2,1)S(1)}, u32[]{:S(2)}, u32[]{:S(2)}) async-start(bf16[16,4,4,8,128]{4,3,2,1,0:T(8,128)(2,1)} %bitcast.68), calls=%async_computation.1 | async-start | bytes 1048576 | tf_op jit(solution)/shard_map/all_to_all | solution.py:42
  133.9 15.3 %copy-start.6 = (bf16[4,4,8,128]{3,2,1,0:T(8,128)(2,1)}, bf16[4,4,8,128]{3,2,1,0:T(8,128)(2,1)S(1)}, u32[]{:S(2)}) copy-start(bf16[4,4,8,128]{3,2,1,0:T(8,128)(2,1)S(1)} %reduce_sum.49) | copy-start | bytes 98308
  134.9 13.5 %all-to-all-start.3 = ((f32[16,4,4,128]{3,2,1,0:T(4,128)}), f32[16,4,4,128]{3,2,1,0:T(4,128)S(1)}, u32[]{:S(2)}, u32[]{:S(2)}) async-start(f32[16,4,4,128]{3,2,1,0:T(4,128)} %broadcast_in_dim.25), calls=%async_computation.3 | async-start | bytes 262144 | tf_op jit(solution)/shard_map/all_to_all | solution.py:9
Sparse Core Ops, SparseCore 0:
  9.8 47.5 all-gather.1
where the time goes:
time: 157 us; the launch traced here: 156 us
  waiting for transfers between devices  73.7 us (47%)
  starting transfers between devices  25.2 us (16%)
  matrix products  20.8 us (13%)
  between operations  14.3 us (9%)
  local copies, waits for them, and re-layouts  11.9 us (8%)
  other arithmetic  10 us (6%)
    all_gather x1, waiting for transfers between devices, per_device(): segment = lax.all_gather(flat_rows, 'tp', axis=1, tiled=True)  42.2 us
    all_to_all x3, starting transfers between devices, from_everyone(): lax.all_to_all(jnp.broadcast_to(shard[None], (count, *shard.shape)), axis...  19.6 us
    all_to_all x3, waiting for transfers between devices, from_everyone(): lax.all_to_all(jnp.broadcast_to(shard[None], (count, *shard.shape)), axis...  18.3 us
    all_to_all x1, waiting for transfers between devices, sent_and_summed(): lax.all_to_all(cut_along(shard, dim, count), axis, 0, 0, tiled=True)  12.6 us
    dot_general x1, matrix products, per_device(): jnp.dot(segment, value_weight, preferred_element_type=jnp.float32)  7.4 us
    dot_general x1, matrix products, per_device(): jnp.dot(segment, forget_weight, preferred_element_type=jnp.float32)  6.97 us
    all_to_all x1, starting transfers between devices, sent_and_summed(): lax.all_to_all(cut_along(shard, dim, count), axis, 0, 0, tiled=True)  5.53 us
    another operation x3, other arithmetic  4.02 us
  transfers between devices with their start and end apart: 5, of which 4 were waited for; matrix products, arithmetic and copies ran while one was open for 12% of the time, Pallas kernels for 0%

commit v1 on v0

v1 whole, which is shorter than its diff:
```python
import functools

import jax
import jax.numpy as jnp
from jax import lax
from jax.experimental import pallas as pl
from jax.experimental.pallas import tpu as pltpu
from jax.sharding import PartitionSpec as P

MESH = pl.DeviceIdType.MESH
F32, BF16 = jnp.float32, jnp.bfloat16
AHEAD = 2


def kernel(
    dims,
    tok,
    fti,
    wf,
    wv,
    wq,
    wg,
    slack,
    damp,
    scale,
    cache_o,
    read_o,
    G,
    Wf,
    Wv,
    Wq,
    Wg,
    X,
    SL,
    DM,
    SC,
    acc,
    U,
    LD,
    DS,
    PJ,
    KC,
    QC,
    NV,
    GT,
    RS_S,
    RS_R,
    TT,
    RD,
    CO,
    FO,
    tok_sem,
    in_sem,
    out_sem,
    ag_s,
    ag_r,
    rs_s,
    rs_r,
    tt_s,
    tt_r,
    rd_s,
    rd_r,
    pj_s,
    pj_r,
):
    NX, NSP, NQ, NH, LB, DB, HD, ROWS, SLAB = dims
    HALF = LB // 2
    CH = NH * HD
    gr = lax.axis_index("gr")
    sp = lax.axis_index("sp")
    tp = lax.axis_index("tp")
    x, c = tp // 2, tp % 2
    xl, xr, xo = (x + NX - 1) % NX, (x + 1) % NX, (x + 2) % NX
    sib = tp + 1 - 2 * c
    left, right, opp = 2 * xl + c, 2 * xr + c, 2 * xo + c
    left_s, right_s, opp_s = 2 * xl + 1 - c, 2 * xr + 1 - c, 2 * xo + 1 - c

    def tp_dev(t):
        return (gr, sp, t)

    def sp_dev(s):
        return (gr, s, tp)

    def tok_load(q):
        return pltpu.make_async_copy(tok.at[q], G.at[q, tp], tok_sem.at[q])

    loads = [
        pltpu.make_async_copy(src, dst, in_sem.at[i])
        for i, (src, dst) in enumerate(
            (
                (fti, X),
                (wq, Wq),
                (wg, Wg),
                (wf, Wf),
                (wv, Wv),
                (slack, SL),
                (damp, DM),
                (scale, SC),
            )
        )
    ]
    for q in range(NQ):
        tok_load(q).start()
    for copy in loads:
        copy.start()

    barrier = pltpu.get_barrier_semaphore()
    for t in (left, right, sib):
        pl.semaphore_signal(barrier, inc=1, device_id=tp_dev(t), device_id_type=MESH)

    def greet(k, carry):
        pl.semaphore_signal(
            barrier, inc=1, device_id=sp_dev((sp + k) % NSP), device_id_type=MESH
        )
        return carry

    lax.fori_loop(1, NSP, greet, 0)
    pl.semaphore_wait(barrier, 3 + NSP - 1)

    def ag(q, i, slot, part, dev):
        ref = G.at[q, slot]
        if part is not None:
            ref = G.at[q, slot, pl.ds(part * HALF, HALF)]
        return pltpu.make_async_remote_copy(
            src_ref=ref,
            dst_ref=ref,
            send_sem=ag_s.at[q, i],
            recv_sem=ag_r.at[q, i],
            device_id=tp_dev(dev),
            device_id_type=MESH,
        )

    def send_own(q):
        ag(q, 0, tp, None, right).start()
        ag(q, 1, tp, None, left).start()
        ag(q, 2, tp, None, sib).start()

    for q in range(AHEAD):
        tok_load(q).wait()
        send_own(q)

    for copy in loads[:5]:
        copy.wait()
    own_rows = pl.ds(sp * SLAB, SLAB)
    xv = X[...]

    def small(w):
        return jnp.dot(xv, w, preferred_element_type=F32)

    PJ[sp, 0:NQ, 0:CH] = small(Wq[...])
    PJ[sp, 0:NQ, CH : 2 * CH] = small(Wg[...])
    PJ[sp, NQ : 2 * NQ, 0:CH] = small(Wf[own_rows, :])
    PJ[sp, NQ : 2 * NQ, CH : 2 * CH] = small(Wv[own_rows, :])

    def spread(ref_of, ssem, rsem, peer):
        return pltpu.make_async_remote_copy(
            src_ref=ref_of(0),
            dst_ref=ref_of(1),
            send_sem=ssem,
            recv_sem=rsem,
            device_id=sp_dev(peer),
            device_id_type=MESH,
        )

    def pj_send(k, carry):
        p = (sp + k) % NSP
        spread(lambda _: PJ.at[sp], pj_s.at[p], pj_r.at[sp], p).start()
        return carry

    lax.fori_loop(1, NSP, pj_send, 0)

    for copy in loads[5:]:
        copy.wait()
    upper = lax.broadcasted_iota(jnp.int32, (LB, LB), 1) > lax.broadcasted_iota(
        jnp.int32, (LB, LB), 0
    )
    U[...] = jnp.where(upper, 1.0, 0.0).astype(BF16)

    def later_damping(q, carry):
        dq = DM[q]
        DS[q] = jnp.broadcast_to(jnp.sum(dq, axis=1, keepdims=True), (NH, HD))
        for h in range(NH):
            r = jnp.broadcast_to(dq[h : h + 1, :], (HD, LB))
            total = None
            for _ in range(3):
                part = r.astype(BF16)
                r = r - part.astype(F32)
                term = lax.dot_general(
                    U[...], part, (((1,), (1,)), ((), ())), preferred_element_type=F32
                )
                total = term if total is None else total + term
            LD[q, h] = total
        return carry

    lax.fori_loop(0, NQ, later_damping, 0)

    own_lane = (
        lax.broadcasted_iota(jnp.int32, (ROWS, HD), 1)
        == lax.broadcasted_iota(jnp.int32, (ROWS, HD), 0) + sp * ROWS
    )

    def own_column(row):
        picked = jnp.where(own_lane, jnp.broadcast_to(row, (ROWS, HD)), 0.0)
        return jnp.sum(picked, axis=1, keepdims=True)

    def multiply(q, par, xi, first):
        a0, a1 = G[q, 2 * xi], G[q, 2 * xi + 1]
        r0, r1 = pl.ds(xi * (2 * DB), DB), pl.ds(xi * (2 * DB) + DB, DB)
        for n, w in enumerate((Wf, Wv)):
            r = jnp.dot(a0, w[r0, :], preferred_element_type=F32)
            r += jnp.dot(a1, w[r1, :], preferred_element_type=F32)
            for h in range(NH):
                piece = r[:, h * HD : (h + 1) * HD]
                if first:
                    acc[par, n, h] = piece
                else:
                    acc[par, n, h] += piece

    def stage_a(q):
        par = q % 2
        ag(q, 2, sib, None, sib).wait_recv()
        multiply(q, par, x, True)
        ag(q, 0, left, None, left).wait_recv()
        ag(q, 5, left, 0, right).start()
        ag(q, 3, left, None, sib).start()
        ag(q, 1, right, None, right).wait_recv()
        ag(q, 6, right, 1, left).start()
        ag(q, 4, right, None, sib).start()

        @pl.when(q + AHEAD < NQ)
        def _():
            tok_load(q + AHEAD).wait()
            send_own(q + AHEAD)

        ag(q, 3, left_s, None, sib).wait_recv()
        multiply(q, par, xl, False)
        ag(q, 4, right_s, None, sib).wait_recv()
        multiply(q, par, xr, False)

    def rs_copy(q, p):
        return pltpu.make_async_remote_copy(
            src_ref=RS_S.at[q, p],
            dst_ref=RS_R.at[q, sp],
            send_sem=rs_s.at[q, p],
            recv_sem=rs_r.at[q, sp],
            device_id=sp_dev(p),
            device_id_type=MESH,
        )

    def tt_copy(q, p):
        return spread(lambda _: TT.at[q, sp], tt_s.at[q, p], tt_r.at[q, sp], p)

    def rd_copy(q, p):
        return spread(lambda _: RD.at[q, sp], rd_s.at[q, p], rd_r.at[q, sp], p)

    def stage_b(q):
        par = q % 2
        ag(q, 5, opp, 0, right).wait_recv()
        ag(q, 7, opp, 0, sib).start()
        ag(q, 6, opp, 1, left).wait_recv()
        ag(q, 8, opp, 1, sib).start()
        ag(q, 7, opp_s, 0, sib).wait_recv()
        ag(q, 8, opp_s, 1, sib).wait_recv()
        multiply(q, par, xo, False)
        totals, blocks = [], []
        for h in range(NH):
            f = acc[par, 0, h].astype(BF16).astype(F32)
            k = SL[h : h + 1, :] * jax.nn.sigmoid(-f)
            d = jnp.log1p(-k)
            d1 = d.astype(BF16)
            d2 = (d - d1.astype(F32)).astype(BF16)
            sums = jnp.dot(
                U[...], jnp.concatenate([d1, d2], axis=1), preferred_element_type=F32
            )
            later = sums[:, :HD] + sums[:, HD:] + LD[q, h]
            w = (k * jnp.exp(later)).astype(BF16)
            v = acc[par, 1, h].astype(BF16)
            s = lax.dot_general(w, v, (((0,), (0,)), ((), ())), preferred_element_type=F32)
            blocks.append(s.reshape(NSP, ROWS, HD))
            totals.append(jnp.sum(d, axis=0, keepdims=True))
        TT[q, sp] = jnp.concatenate(totals, axis=0) + DS[q]
        RS_S[q] = jnp.concatenate(blocks, axis=1).astype(BF16)

        def send(k, carry):
            p = (sp + k) % NSP
            tt_copy(q, p).start()
            rs_copy(q, p).start()
            return carry

        lax.fori_loop(1, NSP, send, 0)

    def wait_peers(copy_from):
        def wait(k, carry):
            copy_from((sp + k) % NSP).wait_recv()
            return carry

        lax.fori_loop(1, NSP, wait, 0)

    def from_peer(ref, rsem, ssem, p):
        return pltpu.make_async_remote_copy(
            src_ref=ref,
            dst_ref=ref,
            send_sem=ssem,
            recv_sem=rsem,
            device_id=sp_dev(p),
            device_id_type=MESH,
        )

    def new_token():
        wait_peers(lambda p: from_peer(PJ.at[p], pj_r.at[p], pj_s.at[p], p))
        total = PJ[0]
        for j in range(1, NSP):
            total = total + PJ[j]
        total = total.astype(BF16).astype(F32)
        GT[...] = total[0:NQ, CH : 2 * CH]
        for h in range(NH):
            lanes = slice(h * HD, (h + 1) * HD)
            qh = total[0:NQ, lanes]
            kh = SL[h : h + 1, :] * jax.nn.sigmoid(-total[NQ : 2 * NQ, lanes])
            vh = total[NQ : 2 * NQ, CH + h * HD : CH + (h + 1) * HD]
            for q in range(NQ):
                KC[q, h] = jnp.broadcast_to(own_column(kh[q : q + 1, :]), (ROWS, HD))
                QC[q, h] = jnp.broadcast_to(own_column(qh[q : q + 1, :]), (ROWS, HD))
                NV[q, h : h + 1, :] = vh[q : q + 1, :]

    def cache_out(q):
        return pltpu.make_async_copy(CO.at[q], cache_o.at[q], out_sem.at[q])

    def stage_c(q):
        wait_peers(lambda p: from_peer(TT.at[q, p], tt_r.at[q, p], tt_s.at[q, p], p))
        wait_peers(lambda p: from_peer(RS_R.at[q, p], rs_r.at[q, p], rs_s.at[q, p], p))
        RS_R[q, sp] = RS_S[q, sp]
        later = jnp.zeros((NH, HD), F32)
        sums = [jnp.zeros((ROWS, HD), F32) for _ in range(NH)]
        for j in reversed(range(NSP)):
            decay = jnp.exp(later)
            block = RS_R[q, j].astype(F32)
            for h in range(NH):
                sums[h] = sums[h] + own_column(decay[h : h + 1, :]) * block[
                    h * ROWS : (h + 1) * ROWS, :
                ]
            later = later + TT[q, j]
        parts = []
        for h in range(NH):
            kept = sums[h].astype(BF16)
            CO[q, h] = kept
            updated = (1.0 - KC[q, h]) * kept.astype(F32) + KC[q, h] * NV[q, h : h + 1, :]
            parts.append(jnp.sum(QC[q, h] * updated, axis=0, keepdims=True))
        RD[q, sp] = jnp.concatenate(parts, axis=0)

        def send(k, carry):
            rd_copy(q, (sp + k) % NSP).start()
            return carry

        lax.fori_loop(1, NSP, send, 0)
        cache_out(q).start()

    def step(it, carry):
        @pl.when(it < NQ)
        def _():
            stage_a(it)

        @pl.when(jnp.logical_and(it >= 1, it <= NQ))
        def _():
            stage_b(it - 1)

        @pl.when(it == 2)
        def _():
            new_token()

        @pl.when(it >= 2)
        def _():
            stage_c(it - 2)

        return carry

    lax.fori_loop(0, NQ + 2, step, 0)

    rows = []
    for q in range(NQ):
        wait_peers(lambda p: from_peer(RD.at[q, p], rd_r.at[q, p], rd_s.at[q, p], p))
        total = RD[q, 0]
        for j in range(1, NSP):
            total = total + RD[q, j]
        spread_of = jnp.mean(total * total, axis=-1, keepdims=True)
        scaled = total * lax.rsqrt(spread_of + 1e-06) * SC[...]
        rows.append(
            jnp.concatenate([scaled[h : h + 1, :] for h in range(NH)], axis=1)
        )
    FO[...] = (jnp.concatenate(rows, axis=0) * jax.nn.silu(GT[...])).astype(BF16)
    read_out = pltpu.make_async_copy(FO, read_o, out_sem.at[NQ])
    read_out.start()

    def drain_ag(q, carry):
        for i, part, dev in (
            (0, None, right),
            (1, None, left),
            (2, None, sib),
            (3, None, sib),
            (4, None, sib),
            (5, 0, right),
            (6, 1, left),
            (7, 0, sib),
            (8, 1, sib),
        ):
            ag(q, i, tp, part, dev).wait_send()
        cache_out(q).wait()

        def drain(k, inner):
            p = (sp + k) % NSP
            tt_copy(q, p).wait_send()
            rs_copy(q, p).wait_send()
            rd_copy(q, p).wait_send()
            return inner

        lax.fori_loop(1, NSP, drain, 0)
        return carry

    lax.fori_loop(0, NQ, drain_ag, 0)

    def drain_pj(k, carry):
        p = (sp + k) % NSP
        spread(lambda _: PJ.at[sp], pj_s.at[p], pj_r.at[sp], p).wait_send()
        return carry

    lax.fori_loop(1, NSP, drain_pj, 0)
    read_out.wait()


def per_device(tok, fti, wf, wv, wq, wg, slack, damp, scale):
    nq, lb, db = tok.shape
    hd = scale.shape[0]
    nh = damp.shape[2]
    nsp, ntp = lax.axis_size("sp"), lax.axis_size("tp")
    rows, slab, ch = hd // nsp, fti.shape[1], nh * hd
    dims = (ntp // 2, nsp, nq, nh, lb, db, hd, rows, slab)
    dma = pltpu.SemaphoreType.DMA
    V = pltpu.VMEM
    return pl.pallas_call(
        functools.partial(kernel, dims),
        out_shape=(
            jax.ShapeDtypeStruct((nq, nh, rows, hd), BF16),
            jax.ShapeDtypeStruct((nq, ch), BF16),
        ),
        in_specs=[pl.BlockSpec(memory_space=pl.ANY)] * 9,
        out_specs=[pl.BlockSpec(memory_space=pl.ANY)] * 2,
        scratch_shapes=[
            V((nq, ntp, lb, db), BF16),
            V(wf.shape, BF16),
            V(wv.shape, BF16),
            V(wq.shape, BF16),
            V(wg.shape, BF16),
            V(fti.shape, BF16),
            V((nh, hd), F32),
            V((nq, nh, lb), F32),
            V((1, hd), F32),
            V((2, 2, nh, lb, hd), F32),
            V((lb, lb), BF16),
            V((nq, nh, lb, hd), F32),
            V((nq, nh, hd), F32),
            V((nsp, 2 * nq, 2 * ch), F32),
            V((nq, nh, rows, hd), F32),
            V((nq, nh, rows, hd), F32),
            V((nq, nh, hd), F32),
            V((nq, ch), F32),
            V((nq, nsp, nh * rows, hd), BF16),
            V((nq, nsp, nh * rows, hd), BF16),
            V((nq, nsp, nh, hd), F32),
            V((nq, nsp, nh, hd), F32),
            V((nq, nh, rows, hd), BF16),
            V((nq, ch), BF16),
            dma((nq,)),
            dma((8,)),
            dma((nq + 1,)),
            dma((nq, 9)),
            dma((nq, 9)),
            dma((nq, nsp)),
            dma((nq, nsp)),
            dma((nq, nsp)),
            dma((nq, nsp)),
            dma((nq, nsp)),
            dma((nq, nsp)),
            dma((nsp,)),
            dma((nsp,)),
        ],
        compiler_params=pltpu.CompilerParams(
            collective_id=0, has_side_effects=True, vmem_limit_bytes=60 << 20
        ),
        name="linear_state",
    )(
        tok,
        fti,
        wf,
        wv,
        wq,
        wg,
        slack.reshape(nh, hd),
        jnp.swapaxes(damp, 1, 2),
        scale.reshape(1, hd),
    )


def solution(mesh):
    placed = (
        P("gr", "sp", "tp"),
        P("gr", "sp"),
        P(None, "tp"),
        P(None, "tp"),
        P("sp", "tp"),
        P("sp", "tp"),
        P("tp"),
        P("gr", "sp", "tp"),
        P(),
    )
    return jax.shard_map(
        per_device,
        mesh=mesh,
        in_specs=placed,
        out_specs=(P("gr", "tp", "sp", None), P("gr", "tp")),
        check_vma=False,
    )
```

time: 157 us -> 63.2 us (0.40)
  waiting for transfers between devices: 73.7 us -> 0 us
  Pallas kernels: 0 us -> 59.7 us
  starting transfers between devices: 25.2 us -> 0 us
  matrix products: 20.8 us -> 0 us
  between operations: 14.3 us -> 0.64 us
  other arithmetic: 10 us -> 0 us
  local copies, waits for them, and re-layouts: 11.9 us -> 2.65 us
    pallas_call x0 -> x1, Pallas kernels: none -> 59.7 us  [per_device(): pl.pallas_call(functools.partial(kernel, dims), out_shape=(jax.ShapeDtype...]
    all_gather x1 -> x0, waiting for transfers between devices: 42.2 us -> none  [per_device(): segment = lax.all_gather(flat_rows, 'tp', axis=1, tiled=True)]
    all_to_all x4 -> x0, waiting for transfers between devices: 30.9 us -> none  [the longest x3 18.3 us: from_everyone(): lax.all_to_all(jnp.broadcast_to(shard[None], (count, *shard.shape)), axis...]
    all_to_all x4 -> x0, starting transfers between devices: 25.1 us -> none  [the longest x3 19.6 us: from_everyone(): lax.all_to_all(jnp.broadcast_to(shard[None], (count, *shard.shape)), axis...]
    dot_general x8 -> x0, matrix products: 20.8 us -> none  [the longest x1 7.4 us: per_device(): jnp.dot(segment, value_weight, preferred_element_type=jnp.float32)]
    another operation x3 -> x0, other arithmetic: 4.02 us -> none
    reshape x4 -> x0, local copies, waits for them, and re-layouts: 3.86 us -> none  [the longest x1 1.78 us: per_device(): jnp.repeat(additional_damping_exponent, head_dim, axis=2)]
    broadcast_in_dim x4 -> x0, local copies, waits for them, and re-layouts: 3.51 us -> none  [the longest x3 2.54 us: from_everyone(): jnp.broadcast_to(shard[None], (count, *shard.shape))]
  transfers between devices with their start and end apart: 5 -> 0, of which waited for: 4 -> 0; matrix products, arithmetic and copies ran while one was open for 12% -> 0% of each run, Pallas kernels for 0% -> 0%
where the time goes in v1:
time: 63.2 us; the launch traced here: 63 us
  Pallas kernels  59.7 us (94%)
  local copies, waits for them, and re-layouts  2.65 us (4%)
  between operations  0.64 us (1%)
    pallas_call x1, Pallas kernels, per_device(): pl.pallas_call(functools.partial(kernel, dims), out_shape=(jax.ShapeDtype...  59.7 us
    unnamed x2, local copies, waits for them, and re-layouts  2.65 us

profile of v1, /device:TPU:1, one launch (start us, length us, event | category | flops | bytes accessed | tf_op | source)
XLA Modules:
  0.0 63.0 jit_solution(8131322683040698942)
XLA Ops:
  0.6 59.7 %linear_state.1 = (bf16[4,4,8,128]{3,2,1,0:T(8,128)(2,1)}, bf16[4,512]{1,0:T(4,128)(2,1)}) custom-call(bf16[4,192,512]{2,1,0:T(8,128)(2,1)} %tok.1, bf16[4,256]{1,0:T(4,128)(2,1)} %fti.1, bf16[4096,512]{1,0:T(8,128)(2,1)} %wf.1, bf16[4096,512]{1,0:T(8,128)(2,1)} %wv.1, bf16[256,512]{1,0:T(8,128)(2,1)} %wq.1, bf16[256,512]{1,0:T(8,128)(2,1)} %wg.1, ...), custom_call_target="tpu_custom_call" | custom-call | tf_op jit(solution)/shard_map/linear_state/pallas_call | solution.py:439
  60.3 1.4 %copy.13 = bf16[4,4,8,128]{3,2,1,0:T(8,128)(2,1)} copy(bf16[4,4,8,128]{3,2,1,0:T(8,128)(2,1)} %get-tuple-element.4) | data formatting | bytes 65536
  61.7 1.3 %copy.14 = bf16[4,512]{1,0:T(4,128)(2,1)} copy(bf16[4,512]{1,0:T(4,128)(2,1)} %get-tuple-element.5) | data formatting | bytes 8192

commit v2 on v1

v2 whole, which is shorter than its diff:
```python
import functools

import jax
import jax.numpy as jnp
from jax import lax
from jax.experimental import pallas as pl
from jax.experimental.pallas import tpu as pltpu
from jax.sharding import PartitionSpec as P

MESH = pl.DeviceIdType.MESH
F32, BF16 = jnp.float32, jnp.bfloat16
AHEAD = 2


def kernel(
    dims,
    tok,
    fti,
    wf,
    wv,
    wq,
    wg,
    slack,
    damp,
    scale,
    cache_o,
    read_o,
    G,
    Wf,
    Wv,
    Wq,
    Wg,
    X,
    SL,
    DM,
    SC,
    acc,
    KS,
    DD,
    U,
    LD,
    DS,
    PJ,
    QK,
    CV,
    GT,
    SH,
    RS_S,
    RS_R,
    TT,
    RD,
    tok_sem,
    in_sem,
    ready,
    ag_s,
    ag_r,
    rs_s,
    rs_r,
    tt_s,
    tt_r,
    rd_s,
    rd_r,
    pj_s,
    pj_r,
):
    NX, NY, NZ, NQ, NH, LB, DB, HD, ROWS, SLAB = dims
    NSP = NY * NZ
    HALF = LB // 2
    CH = NH * HD
    gr = lax.axis_index("gr")
    sp = lax.axis_index("sp")
    tp = lax.axis_index("tp")
    x, c = tp // 2, tp % 2
    z, y = sp // NY, sp % NY
    xl, xr, xo = (x + NX - 1) % NX, (x + 1) % NX, (x + 2) % NX
    sib = tp + 1 - 2 * c
    left, right, opp = 2 * xl + c, 2 * xr + c, 2 * xo + c
    left_s, right_s, opp_s = 2 * xl + 1 - c, 2 * xr + 1 - c, 2 * xo + 1 - c

    def tp_dev(t):
        return (gr, sp, t)

    def sp_dev(s):
        return (gr, s, tp)

    def tok_load(q):
        return pltpu.make_async_copy(tok.at[q], G.at[q, tp], tok_sem.at[q])

    loads = [
        pltpu.make_async_copy(src, dst, in_sem.at[i])
        for i, (src, dst) in enumerate(
            (
                (fti, X),
                (wq, Wq),
                (wg, Wg),
                (wf, Wf),
                (wv, Wv),
                (slack, SL),
                (damp, DM),
                (scale, SC),
            )
        )
    ]

    def signal(sem, dev):
        pl.semaphore_signal(sem, inc=1, device_id=dev, device_id_type=MESH)

    def signal_y(sem):
        signal(sem, sp_dev(z * NY + (y + 1) % NY))
        signal(sem, sp_dev(z * NY + (y + NY - 1) % NY))

    def signal_z(sem):
        @pl.when(z > 0)
        def _():
            signal(sem, sp_dev(sp - NY))

        @pl.when(z < NZ - 1)
        def _():
            signal(sem, sp_dev(sp + NY))

    near_z = jnp.minimum(z, 1) + jnp.minimum(NZ - 1 - z, 1)

    barrier = pltpu.get_barrier_semaphore()
    for t in (left, right, sib):
        signal(barrier, tp_dev(t))
    signal_y(barrier)
    signal_z(barrier)
    for q in range(NQ):
        tok_load(q).start()
    for copy in loads:
        copy.start()
    pl.semaphore_wait(barrier, 5 + near_z)

    def ag(q, i, slot, part, dev):
        ref = G.at[q, slot]
        if part is not None:
            ref = G.at[q, slot, pl.ds(part * HALF, HALF)]
        return pltpu.make_async_remote_copy(
            src_ref=ref,
            dst_ref=ref,
            send_sem=ag_s.at[q, i],
            recv_sem=ag_r.at[q, i],
            device_id=tp_dev(dev),
            device_id_type=MESH,
        )

    def send_own(q):
        ag(q, 0, tp, None, right).start()
        ag(q, 1, tp, None, left).start()
        ag(q, 2, tp, None, sib).start()

    for q in range(AHEAD):
        tok_load(q).wait()
        send_own(q)

    signal_y(ready.at[0])

    for copy in loads[:5]:
        copy.wait()
    own_rows = pl.ds(sp * SLAB, SLAB)
    xv = X[...]

    def small(w):
        return jnp.dot(xv, w, preferred_element_type=F32)

    PJ[sp, 0:NQ, 0:CH] = small(Wq[...])
    PJ[sp, 0:NQ, CH : 2 * CH] = small(Wg[...])
    PJ[sp, NQ : 2 * NQ, 0:CH] = small(Wf[own_rows, :])
    PJ[sp, NQ : 2 * NQ, CH : 2 * CH] = small(Wv[own_rows, :])

    pl.semaphore_wait(ready.at[0], 2)
    signal_z(ready.at[1])

    for copy in loads[5:]:
        copy.wait()
    upper = lax.broadcasted_iota(jnp.int32, (LB, LB), 1) > lax.broadcasted_iota(
        jnp.int32, (LB, LB), 0
    )
    U[...] = jnp.where(upper, 1.0, 0.0).astype(BF16)
    for step in range(1, NZ - 1):
        pl.semaphore_wait(ready.at[step], near_z)
        signal_z(ready.at[step + 1])
    pl.semaphore_wait(ready.at[NZ - 1], near_z)

    def peers(copy_to):
        for k in range(NSP - 1):
            far = NSP // 2 + (k + 1) // 2 * (1 - 2 * (k % 2))
            copy_to((sp + far) % NSP).start()

    def spread(ref, ssem, rsem, peer):
        return pltpu.make_async_remote_copy(
            src_ref=ref,
            dst_ref=ref,
            send_sem=ssem,
            recv_sem=rsem,
            device_id=sp_dev(peer),
            device_id_type=MESH,
        )

    def all_blocks(ref, ssem, rsem):
        return spread(ref, ssem, rsem, (sp + 1) % NSP)

    def pj_copy(p):
        return spread(PJ.at[sp], pj_s, pj_r, p)

    pj_all = all_blocks(PJ.at[pl.ds(0, NSP - 1)], pj_s, pj_r)
    peers(pj_copy)

    def later_damping(q, carry):
        dq = DM[q]
        DS[q] = jnp.broadcast_to(jnp.sum(dq, axis=1, keepdims=True), (NH, HD))
        for h in range(NH):
            r = jnp.broadcast_to(dq[h : h + 1, :], (HD, LB))
            total = None
            for _ in range(3):
                part = r.astype(BF16)
                r = r - part.astype(F32)
                term = lax.dot_general(
                    U[...], part, (((1,), (1,)), ((), ())), preferred_element_type=F32
                )
                total = term if total is None else total + term
            LD[q, h] = total
        return carry

    lax.fori_loop(0, NQ, later_damping, 0)

    own_lane = (
        lax.broadcasted_iota(jnp.int32, (ROWS, HD), 1)
        == lax.broadcasted_iota(jnp.int32, (ROWS, HD), 0) + sp * ROWS
    )

    def own_column(row):
        picked = jnp.where(own_lane, jnp.broadcast_to(row, (ROWS, HD)), 0.0)
        return jnp.sum(picked, axis=1, keepdims=True)

    def multiply(q, par, xi, first, n):
        w = (Wf, Wv)[n]
        a0, a1 = G[q, 2 * xi], G[q, 2 * xi + 1]
        r0, r1 = pl.ds(xi * (2 * DB), DB), pl.ds(xi * (2 * DB) + DB, DB)
        r = jnp.dot(a0, w[r0, :], preferred_element_type=F32)
        r += jnp.dot(a1, w[r1, :], preferred_element_type=F32)
        for h in range(NH):
            piece = r[:, h * HD : (h + 1) * HD]
            if first:
                acc[par, n, h] = piece
            else:
                acc[par, n, h] += piece

    def stage_a(q):
        par = q % 2
        ag(q, 2, sib, None, sib).wait_recv()
        for n in (0, 1):
            multiply(q, par, x, True, n)
        ag(q, 0, left, None, left).wait_recv()
        ag(q, 5, left, 0, right).start()
        ag(q, 3, left, None, sib).start()
        ag(q, 1, right, None, right).wait_recv()
        ag(q, 6, right, 1, left).start()
        ag(q, 4, right, None, sib).start()

        @pl.when(q + AHEAD < NQ)
        def _():
            tok_load(q + AHEAD).wait()
            send_own(q + AHEAD)

        ag(q, 3, left_s, None, sib).wait_recv()
        for n in (0, 1):
            multiply(q, par, xl, False, n)
        ag(q, 4, right_s, None, sib).wait_recv()
        for n in (0, 1):
            multiply(q, par, xr, False, n)

    def rs_copy(q, p):
        return pltpu.make_async_remote_copy(
            src_ref=RS_S.at[q, p],
            dst_ref=RS_R.at[q, sp],
            send_sem=rs_s.at[q],
            recv_sem=rs_r.at[q],
            device_id=sp_dev(p),
            device_id_type=MESH,
        )

    def rs_all(q):
        return all_blocks(RS_R.at[q, pl.ds(0, NSP - 1)], rs_s.at[q], rs_r.at[q])

    def tt_copy(q, p):
        return spread(TT.at[q, sp], tt_s.at[q], tt_r.at[q], p)

    def tt_all(q):
        return all_blocks(TT.at[q, pl.ds(0, NSP - 1)], tt_s.at[q], tt_r.at[q])

    def rd_copy(q, p):
        return spread(RD.at[q, sp], rd_s.at[q], rd_r.at[q], p)

    def rd_all(q):
        return all_blocks(RD.at[q, pl.ds(0, NSP - 1)], rd_s.at[q], rd_r.at[q])

    def stage_b(q):
        par = q % 2
        ag(q, 5, opp, 0, right).wait_recv()
        ag(q, 7, opp, 0, sib).start()
        ag(q, 6, opp, 1, left).wait_recv()
        ag(q, 8, opp, 1, sib).start()
        ag(q, 7, opp_s, 0, sib).wait_recv()
        ag(q, 8, opp_s, 1, sib).wait_recv()
        multiply(q, par, xo, False, 0)
        totals = []
        for h in range(NH):
            f = acc[par, 0, h].astype(BF16).astype(F32)
            k = SL[h : h + 1, :] * jax.nn.sigmoid(-f)
            d = jnp.log1p(-k)
            d1 = d.astype(BF16)
            KS[h] = k
            DD[h, :, 0:HD] = d1
            DD[h, :, HD : 2 * HD] = (d - d1.astype(F32)).astype(BF16)
            totals.append(jnp.sum(d, axis=0, keepdims=True))
        TT[q, sp] = jnp.concatenate(totals, axis=0) + DS[q]
        peers(lambda p: tt_copy(q, p))
        multiply(q, par, xo, False, 1)
        blocks = []
        for h in range(NH):
            sums = jnp.dot(U[...], DD[h], preferred_element_type=F32)
            later = sums[:, :HD] + sums[:, HD:] + LD[q, h]
            w = (KS[h] * jnp.exp(later)).astype(BF16)
            v = acc[par, 1, h].astype(BF16)
            s = lax.dot_general(w, v, (((0,), (0,)), ((), ())), preferred_element_type=F32)
            SH[par, h * HD : (h + 1) * HD, :] = s.astype(BF16)
            blocks.append(s.reshape(NSP, ROWS, HD))
        RS_S[q] = jnp.concatenate(blocks, axis=1).astype(BF16)
        peers(lambda p: rs_copy(q, p))

    def new_token():
        pj_all.wait_recv()
        total = PJ[0]
        for j in range(1, NSP):
            total = total + PJ[j]
        total = total.astype(BF16).astype(F32)
        GT[...] = total[0:NQ, CH : 2 * CH]
        for q in range(NQ):

            def heads(row, start):
                return jnp.concatenate(
                    [
                        total[row : row + 1, start + h * HD : start + (h + 1) * HD]
                        for h in range(NH)
                    ],
                    axis=0,
                )

            query = heads(q, 0)
            keys = SL[...] * jax.nn.sigmoid(-heads(NQ + q, 0))
            QK[q] = query * (1.0 - keys)
            CV[q] = jnp.sum(query * keys, axis=1, keepdims=True) * heads(NQ + q, CH)

    def stage_r(q):
        par = q % 2
        tt_all(q).wait_recv()
        later = jnp.zeros((NH, HD), F32)
        for j in range(1, NSP):
            later = later + jnp.where(sp < j, TT[q, j], 0.0)
        coef = QK[q] * jnp.exp(later)
        high = coef.astype(BF16).astype(F32)
        both = jnp.concatenate([high, coef - high], axis=0)
        at_head = lax.broadcasted_iota(jnp.int32, (2 * NH, HD), 0) % NH
        spaced = jnp.concatenate(
            [jnp.where(at_head == h, both, 0.0) for h in range(NH)], axis=1
        ).astype(BF16)
        out = jnp.dot(spaced, SH[par], preferred_element_type=F32)
        RD[q, sp] = out[0:NH] + out[NH : 2 * NH]
        peers(lambda p: rd_copy(q, p))

    def stage_c(q):
        later = jnp.zeros((NH, HD), F32)
        columns = [None] * NSP
        for j in reversed(range(NSP)):
            decay = jnp.exp(later)
            columns[j] = [own_column(decay[h : h + 1, :]) for h in range(NH)]
            later = later + TT[q, j]
        rs_all(q).wait_recv()
        RS_R[q, sp] = RS_S[q, sp]
        sums = [jnp.zeros((ROWS, HD), F32) for _ in range(NH)]
        for j in reversed(range(NSP)):
            block = RS_R[q, j].astype(F32)
            for h in range(NH):
                sums[h] = sums[h] + columns[j][h] * block[h * ROWS : (h + 1) * ROWS, :]
        for h in range(NH):
            cache_o[q, h] = sums[h].astype(BF16)

    def step(it, carry):
        @pl.when(it < NQ)
        def _():
            stage_a(it)

        @pl.when(jnp.logical_and(it >= 1, it <= NQ))
        def _():
            stage_b(it - 1)

        @pl.when(it == 2)
        def _():
            new_token()

        @pl.when(jnp.logical_and(it >= 2, it <= NQ + 1))
        def _():
            stage_r(it - 2)

        @pl.when(it >= 3)
        def _():
            stage_c(it - 3)

        return carry

    lax.fori_loop(0, NQ + 3, step, 0)

    def drain(q, carry):
        for i, part in ((0, None), (1, None), (2, None), (3, None), (4, None)):
            ag(q, i, tp, part, sib).wait_send()
        for i, part in ((5, 0), (6, 1), (7, 0), (8, 1)):
            ag(q, i, tp, part, sib).wait_send()
        tt_all(q).wait_send()
        rs_all(q).wait_send()
        rd_all(q).wait_send()
        return carry

    lax.fori_loop(0, NQ, drain, 0)
    pj_all.wait_send()

    rows = []
    for q in range(NQ):
        rd_all(q).wait_recv()
        total = CV[q]
        for j in range(NSP):
            total = total + RD[q, j]
        spread_of = jnp.mean(total * total, axis=-1, keepdims=True)
        scaled = total * lax.rsqrt(spread_of + 1e-06) * SC[...]
        rows.append(
            jnp.concatenate([scaled[h : h + 1, :] for h in range(NH)], axis=1)
        )
    read_o[...] = (jnp.concatenate(rows, axis=0) * jax.nn.silu(GT[...])).astype(BF16)


def emit(cache, read, cache_o, read_o, sem):
    copies = [
        pltpu.make_async_copy(cache, cache_o, sem.at[0]),
        pltpu.make_async_copy(read, read_o, sem.at[1]),
    ]
    for copy in copies:
        copy.start()
    for copy in copies:
        copy.wait()


def per_device(tok, fti, wf, wv, wq, wg, slack, damp, scale):
    nq, lb, db = tok.shape
    hd = scale.shape[0]
    nh = damp.shape[2]
    nsp, ntp = lax.axis_size("sp"), lax.axis_size("tp")
    ny = 4
    nz = nsp // ny
    rows, slab, ch = hd // nsp, fti.shape[1], nh * hd
    dims = (ntp // 2, ny, nz, nq, nh, lb, db, hd, rows, slab)
    dma = pltpu.SemaphoreType.DMA
    V = pltpu.VMEM
    results = (
        jax.ShapeDtypeStruct((nq, nh, rows, hd), BF16),
        jax.ShapeDtypeStruct((nq, ch), BF16),
    )
    in_vmem = pl.BlockSpec(memory_space=pltpu.VMEM)
    outs = pl.pallas_call(
        functools.partial(kernel, dims),
        out_shape=tuple(V(r.shape, r.dtype) for r in results),
        in_specs=[pl.BlockSpec(memory_space=pl.ANY)] * 9,
        out_specs=[in_vmem] * 2,
        scratch_shapes=[
            V((nq, ntp, lb, db), BF16),
            V(wf.shape, BF16),
            V(wv.shape, BF16),
            V(wq.shape, BF16),
            V(wg.shape, BF16),
            V(fti.shape, BF16),
            V((nh, hd), F32),
            V((nq, nh, lb), F32),
            V((1, hd), F32),
            V((2, 2, nh, lb, hd), F32),
            V((nh, lb, hd), F32),
            V((nh, lb, 2 * hd), BF16),
            V((lb, lb), BF16),
            V((nq, nh, lb, hd), F32),
            V((nq, nh, hd), F32),
            V((nsp, 2 * nq, 2 * ch), F32),
            V((nq, nh, hd), F32),
            V((nq, nh, hd), F32),
            V((nq, ch), F32),
            V((2, nh * hd, hd), BF16),
            V((nq, nsp, nh * rows, hd), BF16),
            V((nq, nsp, nh * rows, hd), BF16),
            V((nq, nsp, nh, hd), F32),
            V((nq, nsp, nh, hd), F32),
            dma((nq,)),
            dma((8,)),
            pltpu.SemaphoreType.REGULAR((nz,)),
            dma((nq, 9)),
            dma((nq, 9)),
            dma((nq,)),
            dma((nq,)),
            dma((nq,)),
            dma((nq,)),
            dma((nq,)),
            dma((nq,)),
            dma,
            dma,
        ],
        compiler_params=pltpu.CompilerParams(
            collective_id=0, has_side_effects=True, vmem_limit_bytes=56 << 20
        ),
        name="linear_state",
    )(
        tok,
        fti,
        wf,
        wv,
        wq,
        wg,
        slack.reshape(nh, hd),
        jnp.swapaxes(damp, 1, 2),
        scale.reshape(1, hd),
    )
    return pl.pallas_call(
        emit,
        out_shape=results,
        in_specs=[in_vmem] * 2,
        out_specs=[pl.BlockSpec(memory_space=pl.ANY)] * 2,
        scratch_shapes=[dma((2,))],
        compiler_params=pltpu.CompilerParams(vmem_limit_bytes=4 << 20),
        name="emit",
    )(*outs)


def solution(mesh):
    placed = (
        P("gr", "sp", "tp"),
        P("gr", "sp"),
        P(None, "tp"),
        P(None, "tp"),
        P("sp", "tp"),
        P("sp", "tp"),
        P("tp"),
        P("gr", "sp", "tp"),
        P(),
    )
    return jax.shard_map(
        per_device,
        mesh=mesh,
        in_specs=placed,
        out_specs=(P("gr", "tp", "sp", None), P("gr", "tp")),
        check_vma=False,
    )
```

time: 63.2 us -> 52 us (0.82)
  Pallas kernels: 59.7 us -> 51.3 us
  local copies, waits for them, and re-layouts: 2.65 us -> 0 us
    pallas_call x1 -> x2, Pallas kernels: 59.7 us -> 51.3 us  [the longest x1 50.7 us: per_device(): pl.pallas_call(functools.partial(kernel, dims), out_shape=tuple((V(r.shap...]
    unnamed x2 -> x0, local copies, waits for them, and re-layouts: 2.65 us -> none
where the time goes in v2:
time: 52 us
  Pallas kernels  51.3 us (99%)
  between operations  0.64 us (1%)
    pallas_call x1, Pallas kernels, per_device(): pl.pallas_call(functools.partial(kernel, dims), out_shape=tuple((V(r.shap...  50.7 us

profile of v2, /device:TPU:1, one launch (start us, length us, event | category | flops | bytes accessed | tf_op | source)
XLA Modules:
  0.0 52.0 jit_solution(17759600192251765445)
XLA Ops:
  0.6 50.7 %linear_state.1 = (bf16[4,4,8,128]{3,2,1,0:T(8,128)(2,1)S(1)}, bf16[4,512]{1,0:T(4,128)(2,1)S(1)}) custom-call(bf16[4,192,512]{2,1,0:T(8,128)(2,1)} %tok.1, bf16[4,256]{1,0:T(4,128)(2,1)} %fti.1, bf16[4096,512]{1,0:T(8,128)(2,1)} %wf.1, bf16[4096,512]{1,0:T(8,128)(2,1)} %wv.1, bf16[256,512]{1,0:T(8,128)(2,1)} %wq.1, bf16[256,512]{1,0:T(8,128)(2,1)} %wg.1, ...), custom_call_target="tpu_custom_call" | custom-call | tf_op jit(solution)/shard_map/linear_state/pallas_call | solution.py:468
  51.3 0.6 %emit.1 = (bf16[4,4,8,128]{3,2,1,0:T(8,128)(2,1)}, bf16[4,512]{1,0:T(4,128)(2,1)}) custom-call(bf16[4,4,8,128]{3,2,1,0:T(8,128)(2,1)S(1)} %get-tuple-element.4.cache, bf16[4,512]{1,0:T(4,128)(2,1)S(1)} %get-tuple-element.5.read), custom_call_target="tpu_custom_call" | custom-call | tf_op jit(solution)/shard_map/emit/pallas_call | solution.py:527

commit v3 on v2

--- a/solution.py
+++ b/solution.py
@@ -9,7 +9,6 @@
 
 MESH = pl.DeviceIdType.MESH
 F32, BF16 = jnp.float32, jnp.bfloat16
-AHEAD = 2
 
 
 def kernel(
@@ -49,6 +48,7 @@
     RS_R,
     TT,
     RD,
+    RW,
     tok_sem,
     in_sem,
     ready,
@@ -120,15 +120,13 @@
 
     near_z = jnp.minimum(z, 1) + jnp.minimum(NZ - 1 - z, 1)
 
+    tok_load(0).start()
     barrier = pltpu.get_barrier_semaphore()
     for t in (left, right, sib):
         signal(barrier, tp_dev(t))
     signal_y(barrier)
     signal_z(barrier)
-    for q in range(NQ):
-        tok_load(q).start()
-    for copy in loads:
-        copy.start()
+    tok_load(1).start()
     pl.semaphore_wait(barrier, 5 + near_z)
 
     def ag(q, i, slot, part, dev):
@@ -144,35 +142,30 @@
             device_id_type=MESH,
         )
 
-    def send_own(q):
-        ag(q, 0, tp, None, right).start()
-        ag(q, 1, tp, None, left).start()
+    def send_first(q):
+        ag(q, 0, tp, 0, right).start()
+        ag(q, 1, tp, 1, left).start()
         ag(q, 2, tp, None, sib).start()
 
-    for q in range(AHEAD):
-        tok_load(q).wait()
-        send_own(q)
+    def send_second(q):
+        ag(q, 9, tp, 1, right).start()
+        ag(q, 10, tp, 0, left).start()
+
+    tok_load(0).wait()
+    send_first(0)
+    send_second(0)
+    tok_load(1).wait()
+    send_first(1)
+    for copy in loads:
+        copy.start()
+    for q in range(2, NQ):
+        tok_load(q).start()
 
     signal_y(ready.at[0])
-
-    for copy in loads[:5]:
-        copy.wait()
-    own_rows = pl.ds(sp * SLAB, SLAB)
-    xv = X[...]
-
-    def small(w):
-        return jnp.dot(xv, w, preferred_element_type=F32)
-
-    PJ[sp, 0:NQ, 0:CH] = small(Wq[...])
-    PJ[sp, 0:NQ, CH : 2 * CH] = small(Wg[...])
-    PJ[sp, NQ : 2 * NQ, 0:CH] = small(Wf[own_rows, :])
-    PJ[sp, NQ : 2 * NQ, CH : 2 * CH] = small(Wv[own_rows, :])
 
     pl.semaphore_wait(ready.at[0], 2)
     signal_z(ready.at[1])
 
-    for copy in loads[5:]:
-        copy.wait()
     upper = lax.broadcasted_iota(jnp.int32, (LB, LB), 1) > lax.broadcasted_iota(
         jnp.int32, (LB, LB), 0
     )
@@ -204,25 +197,41 @@
         return spread(PJ.at[sp], pj_s, pj_r, p)
 
     pj_all = all_blocks(PJ.at[pl.ds(0, NSP - 1)], pj_s, pj_r)
-    peers(pj_copy)
-
-    def later_damping(q, carry):
-        dq = DM[q]
-        DS[q] = jnp.broadcast_to(jnp.sum(dq, axis=1, keepdims=True), (NH, HD))
-        for h in range(NH):
-            r = jnp.broadcast_to(dq[h : h + 1, :], (HD, LB))
-            total = None
-            for _ in range(3):
-                part = r.astype(BF16)
-                r = r - part.astype(F32)
-                term = lax.dot_general(
-                    U[...], part, (((1,), (1,)), ((), ())), preferred_element_type=F32
-                )
-                total = term if total is None else total + term
-            LD[q, h] = total
-        return carry
-
-    lax.fori_loop(0, NQ, later_damping, 0)
+    def early():
+        for copy in loads[:5]:
+            copy.wait()
+        own_rows = pl.ds(sp * SLAB, SLAB)
+        xv = X[...]
+
+        def small(w):
+            return jnp.dot(xv, w, preferred_element_type=F32)
+
+        PJ[sp, 0:NQ, 0:CH] = small(Wq[...])
+        PJ[sp, 0:NQ, CH : 2 * CH] = small(Wg[...])
+        PJ[sp, NQ : 2 * NQ, 0:CH] = small(Wf[own_rows, :])
+        PJ[sp, NQ : 2 * NQ, CH : 2 * CH] = small(Wv[own_rows, :])
+
+        peers(pj_copy)
+        for copy in loads[5:]:
+            copy.wait()
+
+        def later_damping(q, carry):
+            dq = DM[q]
+            DS[q] = jnp.broadcast_to(jnp.sum(dq, axis=1, keepdims=True), (NH, HD))
+            for h in range(NH):
+                r = jnp.broadcast_to(dq[h : h + 1, :], (HD, LB))
+                total = None
+                for _ in range(3):
+                    part = r.astype(BF16)
+                    r = r - part.astype(F32)
+                    term = lax.dot_general(
+                        U[...], part, (((1,), (1,)), ((), ())), preferred_element_type=F32
+                    )
+                    total = term if total is None else total + term
+                LD[q, h] = total
+            return carry
+
+        lax.fori_loop(0, NQ, later_damping, 0)
 
     own_lane = (
         lax.broadcasted_iota(jnp.int32, (ROWS, HD), 1)
@@ -233,12 +242,7 @@
         picked = jnp.where(own_lane, jnp.broadcast_to(row, (ROWS, HD)), 0.0)
         return jnp.sum(picked, axis=1, keepdims=True)
 
-    def multiply(q, par, xi, first, n):
-        w = (Wf, Wv)[n]
-        a0, a1 = G[q, 2 * xi], G[q, 2 * xi + 1]
-        r0, r1 = pl.ds(xi * (2 * DB), DB), pl.ds(xi * (2 * DB) + DB, DB)
-        r = jnp.dot(a0, w[r0, :], preferred_element_type=F32)
-        r += jnp.dot(a1, w[r1, :], preferred_element_type=F32)
+    def add_up(par, n, r, first):
         for h in range(NH):
             piece = r[:, h * HD : (h + 1) * HD]
             if first:
@@ -246,29 +250,46 @@
             else:
                 acc[par, n, h] += piece
 
-    def stage_a(q):
-        par = q % 2
+    def product(q, slot, n):
+        rows = pl.ds(slot * DB, DB)
+        return jnp.dot(G[q, slot], (Wf, Wv)[n][rows, :], preferred_element_type=F32)
+
+    def multiply(q, par, xi, first):
+        for n in (0, 1):
+            add_up(par, n, product(q, 2 * xi, n) + product(q, 2 * xi + 1, n), first)
+
+    def stage_a1(q):
+        ag(q, 0, left, 0, left).wait_recv()
+        ag(q, 5, left, 0, right).start()
+        ag(q, 3, left, 0, sib).start()
+        ag(q, 1, right, 1, right).wait_recv()
+        ag(q, 6, right, 1, left).start()
+        ag(q, 4, right, 1, sib).start()
+
+        @pl.when(q + 1 < NQ)
+        def _():
+            send_second(q + 1)
+
+        @pl.when(q + 2 < NQ)
+        def _():
+            tok_load(q + 2).wait()
+            send_first(q + 2)
+
+    def stage_own(q):
         ag(q, 2, sib, None, sib).wait_recv()
-        for n in (0, 1):
-            multiply(q, par, x, True, n)
-        ag(q, 0, left, None, left).wait_recv()
-        ag(q, 5, left, 0, right).start()
-        ag(q, 3, left, None, sib).start()
-        ag(q, 1, right, None, right).wait_recv()
-        ag(q, 6, right, 1, left).start()
-        ag(q, 4, right, None, sib).start()
-
-        @pl.when(q + AHEAD < NQ)
-        def _():
-            tok_load(q + AHEAD).wait()
-            send_own(q + AHEAD)
-
-        ag(q, 3, left_s, None, sib).wait_recv()
-        for n in (0, 1):
-            multiply(q, par, xl, False, n)
-        ag(q, 4, right_s, None, sib).wait_recv()
-        for n in (0, 1):
-            multiply(q, par, xr, False, n)
+        multiply(q, q % 2, x, True)
+
+    def stage_a2(q):
+        ag(q, 9, left, 1, left).wait_recv()
+        ag(q, 11, left, 1, sib).start()
+        ag(q, 10, right, 0, right).wait_recv()
+        ag(q, 12, right, 0, sib).start()
+        ag(q, 3, left_s, 0, sib).wait_recv()
+        ag(q, 11, left_s, 1, sib).wait_recv()
+        multiply(q, q % 2, xl, False)
+        ag(q, 4, right_s, 1, sib).wait_recv()
+        ag(q, 12, right_s, 0, sib).wait_recv()
+        multiply(q, q % 2, xr, False)
 
     def rs_copy(q, p):
         return pltpu.make_async_remote_copy(
@@ -301,9 +322,11 @@
         ag(q, 7, opp, 0, sib).start()
         ag(q, 6, opp, 1, left).wait_recv()
         ag(q, 8, opp, 1, sib).start()
+        for n in (0, 1):
+            add_up(par, n, product(q, opp, n), False)
         ag(q, 7, opp_s, 0, sib).wait_recv()
         ag(q, 8, opp_s, 1, sib).wait_recv()
-        multiply(q, par, xo, False, 0)
+        add_up(par, 0, product(q, opp_s, 0), False)
         totals = []
         for h in range(NH):
             f = acc[par, 0, h].astype(BF16).astype(F32)
@@ -316,7 +339,7 @@
             totals.append(jnp.sum(d, axis=0, keepdims=True))
         TT[q, sp] = jnp.concatenate(totals, axis=0) + DS[q]
         peers(lambda p: tt_copy(q, p))
-        multiply(q, par, xo, False, 1)
+        add_up(par, 1, product(q, opp_s, 1), False)
         blocks = []
         for h in range(NH):
             sums = jnp.dot(U[...], DD[h], preferred_element_type=F32)
@@ -386,55 +409,73 @@
         for h in range(NH):
             cache_o[q, h] = sums[h].astype(BF16)
 
-    def step(it, carry):
-        @pl.when(it < NQ)
-        def _():
-            stage_a(it)
-
-        @pl.when(jnp.logical_and(it >= 1, it <= NQ))
-        def _():
-            stage_b(it - 1)
-
-        @pl.when(it == 2)
-        def _():
-            new_token()
-
-        @pl.when(jnp.logical_and(it >= 2, it <= NQ + 1))
-        def _():
-            stage_r(it - 2)
-
-        @pl.when(it >= 3)
-        def _():
-            stage_c(it - 3)
-
-        return carry
-
-    lax.fori_loop(0, NQ + 3, step, 0)
+    def stage_d(q):
+        rd_all(q).wait_recv()
+        total = CV[q]
+        for j in range(NSP):
+            total = total + RD[q, j]
+        spread_of = jnp.mean(total * total, axis=-1, keepdims=True)
+        RW[q] = total * lax.rsqrt(spread_of + 1e-06) * SC[...]
 
     def drain(q, carry):
-        for i, part in ((0, None), (1, None), (2, None), (3, None), (4, None)):
-            ag(q, i, tp, part, sib).wait_send()
-        for i, part in ((5, 0), (6, 1), (7, 0), (8, 1)):
+        for i, part in (
+            (0, 0),
+            (1, 1),
+            (2, None),
+            (3, 0),
+            (4, 1),
+            (5, 0),
+            (6, 1),
+            (7, 0),
+            (8, 1),
+            (9, 1),
+            (10, 0),
+            (11, 1),
+            (12, 0),
+        ):
             ag(q, i, tp, part, sib).wait_send()
         tt_all(q).wait_send()
         rs_all(q).wait_send()
         rd_all(q).wait_send()
         return carry
 
-    lax.fori_loop(0, NQ, drain, 0)
-    pj_all.wait_send()
-
-    rows = []
-    for q in range(NQ):
-        rd_all(q).wait_recv()
-        total = CV[q]
-        for j in range(NSP):
-            total = total + RD[q, j]
-        spread_of = jnp.mean(total * total, axis=-1, keepdims=True)
-        scaled = total * lax.rsqrt(spread_of + 1e-06) * SC[...]
-        rows.append(
-            jnp.concatenate([scaled[h : h + 1, :] for h in range(NH)], axis=1)
-        )
+    def at(it, lag, stage):
+        @pl.when(jnp.logical_and(it >= lag, it < NQ + lag))
+        def _():
+            stage(it - lag)
+
+    def step(it, carry):
+        at(it, 0, stage_a1)
+
+        @pl.when(it == 0)
+        def _():
+            early()
+
+        at(it, 0, stage_own)
+        at(it, 1, stage_b)
+
+        @pl.when(it == 2)
+        def _():
+            new_token()
+
+        at(it, 2, stage_r)
+        at(it, 4, stage_d)
+
+        @pl.when(it == NQ + 2)
+        def _():
+            lax.fori_loop(0, NQ, drain, 0)
+            pj_all.wait_send()
+
+        at(it, 3, stage_c)
+        at(it, 0, stage_a2)
+        return carry
+
+    lax.fori_loop(0, NQ + 4, step, 0)
+
+    rows = [
+        jnp.concatenate([RW[q, h : h + 1, :] for h in range(NH)], axis=1)
+        for q in range(NQ)
+    ]
     read_o[...] = (jnp.concatenate(rows, axis=0) * jax.nn.silu(GT[...])).astype(BF16)
 
 
@@ -495,11 +536,12 @@
             V((nq, nsp, nh * rows, hd), BF16),
             V((nq, nsp, nh, hd), F32),
             V((nq, nsp, nh, hd), F32),
+            V((nq, nh, hd), F32),
             dma((nq,)),
             dma((8,)),
             pltpu.SemaphoreType.REGULAR((nz,)),
-            dma((nq, 9)),
-            dma((nq, 9)),
+            dma((nq, 13)),
+            dma((nq, 13)),
             dma((nq,)),
             dma((nq,)),
             dma((nq,)),

time: 52 us -> 50.1 us (0.963)
  Pallas kernels: 51.3 us -> 49.3 us
    pallas_call x1, Pallas kernels: 50.7 us -> 48.7 us  [per_device(): pl.pallas_call(functools.partial(kernel, dims), out_shape=tuple((V(r.shap...]
where the time goes in v3:
time: 50.1 us; the launch traced here: 50 us
  Pallas kernels  49.3 us (98%)
  between operations  0.64 us (1%)
    pallas_call x1, Pallas kernels, per_device(): pl.pallas_call(functools.partial(kernel, dims), out_shape=tuple((V(r.shap...  48.7 us

profile of v3, /device:TPU:1, one launch (start us, length us, event | category | flops | bytes accessed | tf_op | source)
XLA Modules:
  0.0 50.0 jit_solution(14696004166958903243)
XLA Ops:
  0.6 48.7 %linear_state.1 = (bf16[4,4,8,128]{3,2,1,0:T(8,128)(2,1)S(1)}, bf16[4,512]{1,0:T(4,128)(2,1)S(1)}) custom-call(bf16[4,192,512]{2,1,0:T(8,128)(2,1)} %tok.1, bf16[4,256]{1,0:T(4,128)(2,1)} %fti.1, bf16[4096,512]{1,0:T(8,128)(2,1)} %wf.1, bf16[4096,512]{1,0:T(8,128)(2,1)} %wv.1, bf16[256,512]{1,0:T(8,128)(2,1)} %wq.1, bf16[256,512]{1,0:T(8,128)(2,1)} %wg.1, ...), custom_call_target="tpu_custom_call" | custom-call | tf_op jit(solution)/shard_map/linear_state/pallas_call | solution.py:509
  49.3 0.6 %emit.1 = (bf16[4,4,8,128]{3,2,1,0:T(8,128)(2,1)}, bf16[4,512]{1,0:T(4,128)(2,1)}) custom-call(bf16[4,4,8,128]{3,2,1,0:T(8,128)(2,1)S(1)} %get-tuple-element.4.cache, bf16[4,512]{1,0:T(4,128)(2,1)S(1)} %get-tuple-element.5.read), custom_call_target="tpu_custom_call" | custom-call | tf_op jit(solution)/shard_map/emit/pallas_call | solution.py:569

commit v4 on v3

--- a/solution.py
+++ b/solution.py
@@ -254,10 +254,6 @@
         rows = pl.ds(slot * DB, DB)
         return jnp.dot(G[q, slot], (Wf, Wv)[n][rows, :], preferred_element_type=F32)
 
-    def multiply(q, par, xi, first):
-        for n in (0, 1):
-            add_up(par, n, product(q, 2 * xi, n) + product(q, 2 * xi + 1, n), first)
-
     def stage_a1(q):
         ag(q, 0, left, 0, left).wait_recv()
         ag(q, 5, left, 0, right).start()
@@ -277,19 +273,22 @@
 
     def stage_own(q):
         ag(q, 2, sib, None, sib).wait_recv()
-        multiply(q, q % 2, x, True)
+        for n in (0, 1):
+            add_up(q % 2, n, product(q, tp, n) + product(q, sib, n), True)
 
     def stage_a2(q):
         ag(q, 9, left, 1, left).wait_recv()
         ag(q, 11, left, 1, sib).start()
         ag(q, 10, right, 0, right).wait_recv()
         ag(q, 12, right, 0, sib).start()
+        for n in (0, 1):
+            add_up(q % 2, n, product(q, left, n) + product(q, right, n), False)
         ag(q, 3, left_s, 0, sib).wait_recv()
         ag(q, 11, left_s, 1, sib).wait_recv()
-        multiply(q, q % 2, xl, False)
         ag(q, 4, right_s, 1, sib).wait_recv()
         ag(q, 12, right_s, 0, sib).wait_recv()
-        multiply(q, q % 2, xr, False)
+        for n in (0, 1):
+            add_up(q % 2, n, product(q, left_s, n) + product(q, right_s, n), False)
 
     def rs_copy(q, p):
         return pltpu.make_async_remote_copy(

time: 50.1 us -> 50.3 us (level)
  no operation moved by 1% of the time
where the time goes in v4:
time: 50.3 us; the launch traced here: 50.2 us
  Pallas kernels  49.6 us (99%)
  between operations  0.64 us (1%)
    pallas_call x1, Pallas kernels, per_device(): pl.pallas_call(functools.partial(kernel, dims), out_shape=tuple((V(r.shap...  48.9 us

profile of v4, /device:TPU:1, one launch (start us, length us, event | category | flops | bytes accessed | tf_op | source)
XLA Modules:
  0.0 50.2 jit_solution(12310079929137989131)
XLA Ops:
  0.6 48.9 %linear_state.1 = (bf16[4,4,8,128]{3,2,1,0:T(8,128)(2,1)S(1)}, bf16[4,512]{1,0:T(4,128)(2,1)S(1)}) custom-call(bf16[4,192,512]{2,1,0:T(8,128)(2,1)} %tok.1, bf16[4,256]{1,0:T(4,128)(2,1)} %fti.1, bf16[4096,512]{1,0:T(8,128)(2,1)} %wf.1, bf16[4096,512]{1,0:T(8,128)(2,1)} %wv.1, bf16[256,512]{1,0:T(8,128)(2,1)} %wq.1, bf16[256,512]{1,0:T(8,128)(2,1)} %wg.1, ...), custom_call_target="tpu_custom_call" | custom-call | tf_op jit(solution)/shard_map/linear_state/pallas_call | solution.py:508
  49.6 0.6 %emit.1 = (bf16[4,4,8,128]{3,2,1,0:T(8,128)(2,1)}, bf16[4,512]{1,0:T(4,128)(2,1)}) custom-call(bf16[4,4,8,128]{3,2,1,0:T(8,128)(2,1)S(1)} %get-tuple-element.4.cache, bf16[4,512]{1,0:T(4,128)(2,1)S(1)} %get-tuple-element.5.read), custom_call_target="tpu_custom_call" | custom-call | tf_op jit(solution)/shard_map/emit/pallas_call | solution.py:568
